TPU v7x, 32 devices: a whole 2x2x4 slice. The times are simulated.
32 devices in a mesh: sp: 32 (over z, y, x, core), tp: 1.
Axes of the slice: x: 2, y: 2, z: 4, core: 2. Of those that a mesh axis runs over, the one named last changes fastest.
Arguments:
- queries: bfloat16 [4096, 2048], P('sp', 'tp'), may hold values from -6 to 6
- forget_logits: bfloat16 [2, 4096, 2048], P(None, 'sp', 'tp'), may hold values from -7.5 to 7.5
- value_matrix: bfloat16 [4096, 2048], P('sp', 'tp'), may hold values from -6 to 6
- output_gate_logits: bfloat16 [4096, 2048], P('sp', 'tp'), may hold values from -6 to 6
- forget_slack: float32 [2048], P('tp'), may hold values from 0.00012207031 to 0.07
- spike_log_forget: float32 [4096, 16], P('sp', 'tp'), may hold values from -2.8 to 0, as said below
- head_norm_gain: bfloat16 [128], replicated, may hold values from 0.099609375 to 1.8984375
- output_weight: bfloat16 [2048, 2048], P('tp'), may hold values from -0.125 to 0.125
- residual: bfloat16 [4096, 2048], P('sp'), may hold values from -6 to 6
- mixer_norm_gain: bfloat16 [2048], replicated, may hold values from 0.099609375 to 1.8984375
- mixer_gate_weight: bfloat16 [2048, 5632], P('sp', 'tp'), may hold values from -0.125 to 0.125
- mixer_up_weight: bfloat16 [2048, 5632], P('sp', 'tp'), may hold values from -0.125 to 0.125
- mixer_down_weight: bfloat16 [5632, 2048], P('tp', 'sp'), may hold values from -0.078125 to 0.078125
Outputs:
- layer_out: bfloat16 [4096, 2048], P(('sp', 'tp'))
Inputs may be any that keep to these rules, and one draw needn't show every extreme that they name: `spike_log_forget`: zero at all but a few tokens.
All inputs are finite; a program needn't handle non-finite values.
Results may differ from a plain program's by a relative error of at most 0.015.
Values may be sent and summed in bfloat16 or wider, within the bound.
A program may use at most 192 MiB of HBM per device.

v0:
```python
import jax
import jax.numpy as jnp
from jax import lax
from jax.sharding import PartitionSpec as P

BLOCK = 128


NORM_EPS = 1e-06
BEST_PRECISION = lax.Precision.HIGHEST


def entering(array, axis, join, neutral, backward):
    count = lax.axis_size(axis)
    place = lax.axis_index(axis)
    ahead = count - 1 - place if backward else place
    gathered = jax.tree.map(
        lambda a, kind: lax.all_gather(a.astype(kind), axis), array, (jnp.bfloat16, jnp.bfloat16)
    )
    state = jax.tree.map(lambda a, e: jnp.zeros_like(a) + jnp.asarray(e, a.dtype), array, neutral)

    def one(turn, state):
        source = count - 1 - turn if backward else turn
        return join(
            state,
            jax.tree.map(
                lambda a, own: lax.dynamic_index_in_dim(a, source, 0, False).astype(own.dtype),
                gathered,
                array,
            ),
        )

    return lax.fori_loop(0, ahead, one, state)


def rms_scale(entries, gain_vec):
    return (
        entries
        * lax.rsqrt(jnp.mean(entries * entries, axis=-1, keepdims=True) + NORM_EPS)
        * gain_vec.astype(jnp.float32)
    )


def reverse_rows(tensor):
    return jnp.flip(tensor, 0)


def local_sweep(query_f, key_f, decay_f, value_f):
    row_count, heads_present, head_width = query_f.shape
    blocks_count = row_count // BLOCK
    tri_mask = jnp.tril(jnp.ones((BLOCK, BLOCK), bool))

    def to_blocks(tensor):
        return tensor.reshape(blocks_count, BLOCK, heads_present, head_width)

    def advance(carried, segment):
        state_now, offset = carried
        query_seg, key_seg, decay_seg, value_seg = segment
        running = jnp.cumsum(decay_seg, axis=0)
        query_scaled = query_seg * jnp.exp(running)
        key_scaled = key_seg * jnp.exp(-running)
        scores = jnp.einsum("thd,shd->hts", query_scaled, key_scaled, precision=BEST_PRECISION)
        scores = jnp.where(tri_mask[None], scores, 0.0)
        result = jnp.einsum("hts,shv->thv", scores, value_seg, precision=BEST_PRECISION)
        result = result + jnp.einsum(
            "thd,hdv->thv", query_scaled, state_now, precision=BEST_PRECISION
        )
        final_log = running[-1]
        state_next = jnp.exp(final_log)[:, :, None] * state_now + jnp.einsum(
            "shd,shv->hdv",
            key_seg * jnp.exp(final_log[None] - running),
            value_seg,
            precision=BEST_PRECISION,
        )
        reach = query_seg * jnp.exp(running + offset)
        return ((state_next, offset + final_log), (result, reach))

    initial = (
        jnp.zeros((heads_present, head_width, head_width), jnp.float32),
        jnp.zeros((heads_present, head_width), jnp.float32),
    )
    (state_end, offset_end), (results, reaches) = lax.scan(
        advance,
        initial,
        (to_blocks(query_f), to_blocks(key_f), to_blocks(decay_f), to_blocks(value_f)),
    )
    shape_back = (row_count, heads_present, head_width)
    return (
        results.reshape(shape_back),
        reaches.reshape(shape_back),
        state_end,
        jnp.exp(offset_end),
    )


def chain(earlier, latter):
    return (earlier[0] * latter[0], latter[0][..., None] * earlier[1] + latter[1])


def local(
    queries,
    forget_logits,
    value_matrix,
    output_gate_logits,
    forget_slack,
    spike_log_forget,
    head_norm_gain,
    output_weight,
    residual,
    mixer_norm_gain,
    mixer_gate_weight,
    mixer_up_weight,
    mixer_down_weight,
):
    row_count = queries.shape[0]
    heads_present = spike_log_forget.shape[1]
    head_width = queries.shape[1] // heads_present
    query_f = (jax.nn.silu(queries.astype(jnp.float32)) * head_width ** (-0.5)).reshape(
        row_count, heads_present, head_width
    )
    value_f = value_matrix.astype(jnp.float32).reshape(row_count, heads_present, head_width)
    gate_random_key = (forget_slack * jax.nn.sigmoid(-forget_logits.astype(jnp.float32))).reshape(
        2, row_count, heads_present, head_width
    )
    decay_logarithm = jnp.log1p(-gate_random_key) + spike_log_forget[None, :, :, None]
    fore_local, fore_reach, fore_state, fore_total = local_sweep(
        query_f, gate_random_key[0], decay_logarithm[0], value_f
    )
    back_local, back_reach, back_state, back_total = local_sweep(
        reverse_rows(query_f),
        reverse_rows(gate_random_key[1]),
        reverse_rows(decay_logarithm[1]),
        reverse_rows(value_f),
    )
    neutral = (jnp.ones_like(fore_total), jnp.zeros_like(fore_state))
    _, fore_enter = entering((fore_total, fore_state), "sp", chain, neutral, False)
    _, back_enter = entering((back_total, back_state), "sp", chain, neutral, True)
    fore_out = fore_local + jnp.einsum(
        "thd,hdv->thv", fore_reach, fore_enter, precision=BEST_PRECISION
    )
    back_out = back_local + jnp.einsum(
        "thd,hdv->thv", back_reach, back_enter, precision=BEST_PRECISION
    )
    mixture = fore_out + reverse_rows(back_out)
    mixed = (
        rms_scale(mixture, head_norm_gain).reshape(row_count, heads_present * head_width)
        * jax.nn.silu(output_gate_logits.astype(jnp.float32))
    ).astype(jnp.bfloat16)
    part_rows = row_count // lax.axis_size("tp")
    own_start = lax.axis_index("tp") * part_rows
    partial_out = jnp.dot(mixed, output_weight, preferred_element_type=jnp.float32).astype(
        jnp.bfloat16
    )
    mixer_add = lax.psum_scatter(
        lax.optimization_barrier(partial_out).astype(jnp.float32).astype(jnp.bfloat16),
        "tp",
        scatter_dimension=0,
        tiled=True,
    ).astype(jnp.float32)
    own_resid = lax.dynamic_slice_in_dim(residual, own_start, part_rows, 0)
    hidden_state = (own_resid.astype(jnp.float32) + mixer_add).astype(jnp.bfloat16)
    normed_part = rms_scale(hidden_state.astype(jnp.float32), mixer_norm_gain).astype(jnp.bfloat16)
    normed = lax.all_gather(normed_part, "tp", axis=0, tiled=True)
    gate_act = jnp.dot(
        normed,
        lax.all_gather(mixer_gate_weight, "sp", axis=0, tiled=True),
        preferred_element_type=jnp.float32,
    )
    up_act = jnp.dot(
        normed,
        lax.all_gather(mixer_up_weight, "sp", axis=0, tiled=True),
        preferred_element_type=jnp.float32,
    )
    inner = (jax.nn.silu(gate_act) * up_act).astype(jnp.bfloat16)
    lowered = jnp.dot(
        inner,
        lax.all_gather(mixer_down_weight, "sp", axis=1, tiled=True),
        preferred_element_type=jnp.float32,
    )
    lowered_term = lax.optimization_barrier(lowered.astype(jnp.bfloat16)).astype(jnp.float32)
    ffn_add = lax.psum_scatter(
        lowered_term.astype(jnp.bfloat16), "tp", scatter_dimension=0, tiled=True
    ).astype(jnp.float32)
    return (hidden_state.astype(jnp.float32) + ffn_add).astype(jnp.bfloat16)


def solution(mesh):
    placed = (
        P("sp", "tp"),
        P(None, "sp", "tp"),
        P("sp", "tp"),
        P("sp", "tp"),
        P("tp"),
        P("sp", "tp"),
        P(),
        P("tp", None),
        P("sp", None),
        P(),
        P("sp", "tp"),
        P("sp", "tp"),
        P("tp", "sp"),
    )
    return jax.shard_map(
        local, mesh=mesh, in_specs=placed, out_specs=P(("sp", "tp"), None), check_vma=False
    )
```

profile of v0, /device:TPU:1, one launch (start us, length us, event | category | flops | bytes accessed | tf_op | source)
XLA Modules:
  0.0 728.6 jit_solution(13368527805004820737)
XLA Ops:
  6.5 2.4 divide_multiply_fusion
  9.0 1.7 copy.55
  10.7 3.3 bitcast_add_fusion
  14.0 2.3 slice_bitcast_fusion.1
  16.3 2.3 rev.17
  18.5 2.4 fusion.49
  26.6 3.6 exponential_multiply_fusion
  30.2 3.0 fusion.7
  36.1 2.8 bitcast_multiply_fusion
  38.9 2.1 fusion.6
  43.0 44.5 %all_gather.33 = bf16[32,16,128]{2,1,0:T(8,128)(2,1)S(1)} all-gather(bf16[1,16,128]{2,1,0:T(8,128)(2,1)S(1)} %get-tuple-element.230), channel_id=1, replica_groups=mesh['sp'=32,'tp'=1] {'sp'}, dimensions={0}, use_global_device_ids=true | all-gather | bytes 135168 | tf_op jit(solution)/shard_map/all_gather | solution.py:18
  87.6 39.0 %all_gather.30 = bf16[32,16,128]{2,1,0:T(8,128)(2,1)S(1)} all-gather(bf16[1,16,128]{2,1,0:T(8,128)(2,1)S(1)} %get-tuple-element.227), channel_id=1, replica_groups=mesh['sp'=32,'tp'=1] {'sp'}, dimensions={0}, use_global_device_ids=true | all-gather | bytes 135168 | tf_op jit(solution)/shard_map/all_gather | solution.py:18
  126.6 4.1 convolution_select_fusion.1
  131.9 2.8 convolution_select_fusion
  134.7 1.9 convolution_bitcast_fusion.2
  136.6 3.4 fusion.2
  140.0 3.4 fusion.5
  143.4 7.8 %all-gather.16.cloned.1.call-done = bf16[512,128,128]{2,1,0:T(8,128)(2,1)} async-done(((bf16[16,128,128]{2,1,0:T(8,128)(2,1)}), bf16[512,128,128]{2,1,0:T(8,128)(2,1)}) %all-gather.16.cloned.1.call-update) | async-done | bytes 16777232 | tf_op jit(solution)/shard_map/all_gather | solution.py:18
  151.3 48.2 %while.17 = (s32[]{:T(128)}, f32[16,128,128]{2,1,0:T(8,128)S(1)}, s32[]{:T(128)}, bf16[32,16,128]{2,1,0:T(8,128)(2,1)S(1)}, bf16[32,16,128,128]{3,2,1,0:T(8,128)...) while((s32[]{:T(128)}, f32[16,128,128]{2,1,0:T(8,128)S(1)}, s32[]{:T(128)}, ...), condition=%wide.region_5.6_spmd, body=%wide.region_4.5_spmd.sunk | while | flops 788486 | bytes 2642067 | solution.py:33
  151.3 1.5 convert_add_fusion.6
  152.9 1.5 convert_add_fusion.6
  154.5 1.5 convert_add_fusion.6
  156.1 1.5 convert_add_fusion.6
  157.7 1.5 convert_add_fusion.6
  159.3 1.5 convert_add_fusion.6
  160.9 1.6 convert_add_fusion.6
  162.5 1.5 convert_add_fusion.6
  165.7 1.5 convert_add_fusion.6
  167.3 1.5 convert_add_fusion.6
  168.9 1.5 convert_add_fusion.6
  172.1 1.5 convert_add_fusion.6
  173.7 1.5 convert_add_fusion.6
  181.6 1.7 convert_add_fusion.6
  183.4 1.5 convert_add_fusion.6
  188.2 1.6 convert_add_fusion.6
  191.4 1.5 convert_add_fusion.6
  199.5 4.7 fusion.1
  204.2 9.3 %rev.20 = f32[128,16,128]{0,2,1:T(8,128)} reverse(f32[128,16,128]{0,2,1:T(8,128)} %fusion.1), dimensions={0} | reverse | bytes 2097152 | tf_op jit(solution)/shard_map/jit(_flip)/rev | solution.py:45
  213.5 53.7 %all-gather.14.cloned.1.call-done = bf16[512,128,128]{2,1,0:T(8,128)(2,1)} async-done(((bf16[16,128,128]{2,1,0:T(8,128)(2,1)}), bf16[512,128,128]{2,1,0:T(8,128)(2,1)}) %all-gather.14.cloned.1.call-update) | async-done | bytes 16777232 | tf_op jit(solution)/shard_map/all_gather | solution.py:18
  267.3 1.7 while.16
  267.4 1.6 convert_add_fusion.5
  269.0 3.7 multiply_reduce_fusion
  273.8 5.2 convolution_convert_fusion
  279.3 132.9 %all-gather.8.cloned.1.call-done = bf16[2048,5632]{1,0:T(8,128)(2,1)} async-done(((bf16[64,5632]{1,0:T(8,128)(2,1)}), bf16[2048,5632]{1,0:T(8,128)(2,1)}) %all-gather.8.cloned.1.call-update) | async-done | bytes 23068688 | tf_op jit(solution)/shard_map/all_gather | solution.py:166
  412.2 12.4 %fusion.43 = f32[128,5632]{1,0:T(8,128)} fusion(bf16[2048,5632]{1,0:T(8,128)(2,1)} %all-gather.8.cloned.1.call-done, bf16[128,2048]{1,0:T(8,128)(2,1)S(1)} %get-tuple-element.216, f32[2048]{0:T(1024)S(1)} %convert_element_type.124, f32[128]{0:T(128)S(1)} %add_rsqrt_fusion.1), kind=kOutput, calls=%fused_computation.81 | convolution fusion | flops 2953838592 | bytes 26485248 | tf_op jit(solution)/shard_map/dot_general | solution.py:164
  424.6 132.3 %all-gather.10.cloned.1.call-done = bf16[2048,5632]{1,0:T(8,128)(2,1)} async-done(((bf16[64,5632]{1,0:T(8,128)(2,1)}), bf16[2048,5632]{1,0:T(8,128)(2,1)}) %all-gather.10.cloned.1.call-update) | async-done | bytes 23068688 | tf_op jit(solution)/shard_map/all_gather | solution.py:171
  557.0 144.8 %all-gather.12.cloned.1.call-done = bf16[5632,2048]{0,1:T(8,128)(2,1)} async-done(((bf16[5632,64]{0,1:T(8,128)(2,1)}), bf16[5632,2048]{0,1:T(8,128)(2,1)}) %all-gather.12.cloned.1.call-update) | async-done | bytes 23068688 | tf_op jit(solution)/shard_map/all_gather | solution.py:177
  701.7 19.5 %convolution_convert_fusion.1 = bf16[128,2048]{1,0:T(8,128)(2,1)S(1)} fusion(bf16[5632,2048]{0,1:T(8,128)(2,1)} %all-gather.12.cloned.1.call-done, bf16[2048,5632]{1,0:T(8,128)(2,1)} %all-gather.10.cloned.1.call-done, f32[128,5632]{1,0:T(8,128)} %fusion.43, bf16[128,2048]{1,0:T(8,128)(2,1)S(1)} %get-tuple-element.216, f32[2048]{0:T(1024)S(1)} %convert_element_type.124, ...), kind=kOutput, calls=%fused_computation.7 | convolution fusion | flops 5911216128 | bytes 50078208 | tf_op jit(solution)/shard_map/dot_general | solution.py:175
  (103 shorter events, 34.5 us)
Async XLA Ops:
  6.5 19.5 %copy-start = (bf16[128,2048]{1,0:T(8,128)(2,1)S(1)}, bf16[128,2048]{1,0:T(8,128)(2,1)}, u32[]{:S(2)}) copy-start(bf16[128,2048]{1,0:T(8,128)(2,1)} %param.19) | copy-start | bytes 1572868
  6.5 144.6 %all-gather.16.cloned.1.call-start = ((), (), s32[]{:S(2)}) async-start(), calls=%async_computation.4 | async-start | bytes 17301504 | tf_op jit(solution)/shard_map/all_gather | solution.py:18
  8.9 1.7 copy-start.8
  22.3 2.3 copy-start.6
  26.6 3.7 copy-start.2
  33.3 234.0 %all-gather.14.cloned.1.call-start = ((), (), s32[]{:S(2)}) async-start(), calls=%async_computation.3 | async-start | bytes 17301504 | tf_op jit(solution)/shard_map/all_gather | solution.py:18
  38.9 4.1 copy-start.11
  38.9 4.1 copy-start.9
  41.1 371.1 %all-gather.8.cloned.1.call-start = ((), (), s32[]{:S(2)}) async-start(), calls=%async_computation | async-start | bytes 23789568 | tf_op jit(solution)/shard_map/all_gather | solution.py:166
  41.8 515.1 %all-gather.10.cloned.1.call-start = ((), (), s32[]{:S(2)}) async-start(), calls=%async_computation.1 | async-start | bytes 23789568 | tf_op jit(solution)/shard_map/all_gather | solution.py:171
  42.4 659.3 %all-gather.12.cloned.1.call-start = ((), (), s32[]{:S(2)}) async-start(), calls=%async_computation.2 | async-start | bytes 23789568 | tf_op jit(solution)/shard_map/all_gather | solution.py:177
  126.6 5.3 copy-start.5
  130.6 4.0 copy-start.3
  267.3 1.7 copy-start.4
  272.7 1.0 copy-start.10
  273.8 5.2 copy-start.7
  701.7 20.4 %copy-start.1 = (bf16[128,2048]{1,0:T(8,128)(2,1)S(1)}, bf16[128,2048]{1,0:T(8,128)(2,1)}, u32[]{:S(2)}) copy-start(bf16[128,2048]{1,0:T(8,128)(2,1)} %param.19) | copy-start | bytes 1572868
Sparse Core Ops, SparseCore 0:
  33.4 117.7 all-gather.15
  154.0 113.1 all-gather.13
  270.1 142.0 all-gather.7
  414.9 142.0 all-gather.9
  559.6 142.0 all-gather.11
where the time goes:
time: 732 us; the launch traced here: 729 us
  waiting for transfers between devices  473 us (65%)
  blocking collectives  83.5 us (11%)
  other arithmetic  67.5 us (9%)
  matrix products  67.4 us (9%)
  local copies, waits for them, and re-layouts  21.9 us (3%)
  between operations  13.4 us (2%)
    all_gather x1, waiting for transfers between devices, local(): lax.all_gather(mixer_down_weight, 'sp', axis=1, tiled=True)  145 us
    all_gather x1, waiting for transfers between devices, local(): lax.all_gather(mixer_gate_weight, 'sp', axis=0, tiled=True)  133 us
    all_gather x1, waiting for transfers between devices, local(): lax.all_gather(mixer_up_weight, 'sp', axis=0, tiled=True)  132 us
    all_gather x2, blocking collectives, entering(): lax.all_gather(a.astype(kind), axis)  83.5 us
    all_gather x2, waiting for transfers between devices, entering(): lax.all_gather(a.astype(kind), axis)  61.5 us
    add x31, other arithmetic, chain(): latter[0][..., None] * earlier[1] + latter[1]  48.2 us
    dot_general x1, matrix products, local(): jnp.dot(inner, lax.all_gather(mixer_down_weight, 'sp', axis=1, tiled=True...  19.5 us
  transfers between devices with their start and end apart: 5, of which 5 were waited for; matrix products, arithmetic and copies ran while one was open for 15% of the time, Pallas kernels for 0%

commit v1 on v0

v1 whole, which is shorter than its diff:
```python
import functools

import jax
import jax.numpy as jnp
from jax import lax
from jax.experimental import pallas as pl
from jax.experimental.pallas import tpu as pltpu
from jax.sharding import PartitionSpec as P

NORM_EPS = 1e-06
MESH = pl.DeviceIdType.MESH
PAD_ROWS = 16
GROUP = 8


def dot_nt(a, b):
    return lax.dot_general(a, b, (((1,), (1,)), ((), ())), preferred_element_type=jnp.float32)


def dot_tn(a, b):
    return lax.dot_general(a, b, (((0,), (0,)), ((), ())), preferred_element_type=jnp.float32)


def dot_nn(a, b):
    return jnp.dot(a, b, preferred_element_type=jnp.float32)


def silu(x):
    return x * jax.nn.sigmoid(x)


def split_bf16(x):
    high = x.astype(jnp.bfloat16)
    return high, (x - high.astype(jnp.float32)).astype(jnp.bfloat16)


def sweep_kernel(q_ref, f_ref, v_ref, slack_ref, spike_ref, local_ref, reach_ref, state_ref):
    head = pl.program_id(0)
    rows, width = q_ref.shape
    query = silu(q_ref[...].astype(jnp.float32)) * (width ** -0.5)
    value = v_ref[...]
    spikes = spike_ref[...]
    lane = lax.broadcasted_iota(jnp.int32, spikes.shape, 1)
    spike = jnp.sum(jnp.where(lane == head, spikes, 0.0), axis=1, keepdims=True)
    slack = slack_ref[...]
    down = lax.broadcasted_iota(jnp.int32, (rows, rows), 0)
    across = lax.broadcasted_iota(jnp.int32, (rows, rows), 1)
    scores = None
    for way in (0, 1):
        mask = (down >= across) if way == 0 else (down <= across)
        tri = jnp.where(mask, 1.0, 0.0).astype(jnp.bfloat16)
        key = slack * jax.nn.sigmoid(-f_ref[way].astype(jnp.float32))
        decay = jnp.log1p(-key) + spike
        high, low = split_bf16(decay)
        running = dot_nn(tri, high) + dot_nn(tri, low)
        final = running[rows - 1 : rows] if way == 0 else running[0:1]
        query_scaled = (query * jnp.exp(running)).astype(jnp.bfloat16)
        key_scaled = (key * jnp.exp(-running)).astype(jnp.bfloat16)
        key_end = (key * jnp.exp(final - running)).astype(jnp.bfloat16)
        part = jnp.where(mask, dot_nt(query_scaled, key_scaled), 0.0)
        scores = part if scores is None else scores + part
        reach_ref[way] = query_scaled
        state_ref[way, 0, 0:width] = dot_tn(value, key_end).astype(jnp.bfloat16)
        total_high, total_low = split_bf16(jnp.exp(final))
        place = lax.broadcasted_iota(jnp.int32, (PAD_ROWS, width), 0)
        state_ref[way, 0, width : width + PAD_ROWS] = jnp.where(
            place == 0,
            total_high.astype(jnp.float32),
            jnp.where(place == 1, total_low.astype(jnp.float32), 0.0),
        ).astype(jnp.bfloat16)
    local_ref[...] = dot_nn(scores.astype(jnp.bfloat16), value)


def sweep(queries, forget_logits, values, slack, spike):
    rows, columns = queries.shape
    heads = spike.shape[1]
    width = columns // heads
    by_head = pl.BlockSpec((rows, width), lambda h: (0, h))
    return pl.pallas_call(
        sweep_kernel,
        grid=(heads,),
        in_specs=[
            by_head,
            pl.BlockSpec((2, rows, width), lambda h: (0, 0, h)),
            by_head,
            pl.BlockSpec((1, width), lambda h: (0, h)),
            pl.BlockSpec((rows, heads), lambda h: (0, 0)),
        ],
        out_specs=[
            by_head,
            pl.BlockSpec((2, rows, width), lambda h: (0, 0, h)),
            pl.BlockSpec((2, 1, width + PAD_ROWS, width), lambda h: (0, h, 0, 0)),
        ],
        out_shape=[
            jax.ShapeDtypeStruct((rows, columns), jnp.float32),
            jax.ShapeDtypeStruct((2, rows, columns), jnp.bfloat16),
            jax.ShapeDtypeStruct((2, heads, width + PAD_ROWS, width), jnp.bfloat16),
        ],
        cost_estimate=pl.CostEstimate(
            flops=20 * rows * width * columns, bytes_accessed=8 * rows * columns, transcendentals=8 * rows * columns
        ),
        name="sweep",
    )(queries, forget_logits, values, slack.reshape(1, columns), spike)


def greet(axis, others, count):
    barrier = pltpu.get_barrier_semaphore()

    def signal(k, carry):
        pl.semaphore_signal(barrier, inc=1, device_id={axis: others(k)}, device_id_type=MESH)
        return carry

    lax.fori_loop(1, count, signal, 0)
    pl.semaphore_wait(barrier, count - 1)


def exchange_kernel(n, state_ref, enter_ref, held, made, out_sem, in_sem, out_sem2, in_sem2):
    me = lax.axis_index("sp")
    rows = enter_ref.shape[1]

    def other(k):
        return lax.rem(me + k, n)

    greet("sp", other, n)

    def first(k):
        there = other(k)
        return pltpu.make_async_remote_copy(
            src_ref=state_ref.at[there],
            dst_ref=held.at[me],
            send_sem=out_sem.at[k],
            recv_sem=in_sem.at[k],
            device_id={"sp": there},
            device_id_type=MESH,
        )

    def second(k):
        there = other(k)
        return pltpu.make_async_remote_copy(
            src_ref=made.at[there],
            dst_ref=enter_ref.at[me],
            send_sem=out_sem2.at[k],
            recv_sem=in_sem2.at[k],
            device_id={"sp": there},
            device_id_type=MESH,
        )

    def go(copy):
        def start(k, carry):
            copy(k).start()
            return carry

        lax.fori_loop(1, n, start, 0)

    def end(copy):
        def wait(k, carry):
            copy(k).wait()
            return carry

        lax.fori_loop(1, n, wait, 0)

    go(first)
    held[me] = state_ref[me]
    end(first)
    backward = me // (n // 2)

    def step(i, total):
        source = i + backward * (n - 1 - 2 * i)
        made[source] = total.astype(jnp.bfloat16)
        block = held[source].astype(jnp.float32)
        factor = block[rows : rows + 1] + block[rows + 1 : rows + 2]
        return factor * total + block[:rows]

    lax.fori_loop(0, n, step, jnp.zeros(enter_ref.shape[1:], jnp.float32))
    go(second)
    enter_ref[me] = made[me]
    end(second)


def exchange(states):
    n = lax.axis_size("sp")
    ways, heads, padded, width = states.shape
    depth = padded - PAD_ROWS
    cuts = n // (ways * heads)
    rows = depth // cuts
    if cuts > 1:
        body = states[:, :, :depth].reshape(ways, heads, cuts, rows, width)
        tail = jnp.broadcast_to(
            states[:, :, None, depth:], (ways, heads, cuts, PAD_ROWS, width)
        )
        states = jnp.concatenate([body, tail], axis=3)
    entered = pl.pallas_call(
        functools.partial(exchange_kernel, n),
        in_specs=[pl.BlockSpec(memory_space=pltpu.VMEM)],
        out_specs=pl.BlockSpec(memory_space=pltpu.VMEM),
        out_shape=jax.ShapeDtypeStruct((n, rows, width), jnp.bfloat16),
        scratch_shapes=[
            pltpu.VMEM((n, rows + PAD_ROWS, width), jnp.bfloat16),
            pltpu.VMEM((n, rows, width), jnp.bfloat16),
            pltpu.SemaphoreType.DMA((n,)),
            pltpu.SemaphoreType.DMA((n,)),
            pltpu.SemaphoreType.DMA((n,)),
            pltpu.SemaphoreType.DMA((n,)),
        ],
        compiler_params=pltpu.CompilerParams(collective_id=1, has_side_effects=True),
        cost_estimate=pl.CostEstimate(flops=10**8, bytes_accessed=10**8, transcendentals=0),
        name="exchange",
    )(states.reshape(n, rows + PAD_ROWS, width))
    return entered.reshape(ways, heads, depth, width)


def reshard_kernel(g, *refs):
    count = (len(refs) - 3) // 2
    gives, takes = refs[:count], refs[count : 2 * count]
    out_sem, in_sem, own_sem = refs[2 * count :]
    me = lax.axis_index("sp")
    base = me // g * g
    seat = me - base

    def other(k):
        return lax.rem(seat + k, g)

    greet("sp", lambda k: base + other(k), g)
    copies = []
    for k in range(1, g):
        there = other(k)
        for i in range(count):
            copies.append(
                pltpu.make_async_remote_copy(
                    src_ref=gives[i].at[there],
                    dst_ref=takes[i].at[seat],
                    send_sem=out_sem.at[i, k],
                    recv_sem=in_sem.at[i, k],
                    device_id={"sp": base + there},
                    device_id_type=MESH,
                )
            )
            copies[-1].start()
    for i in range(count):
        copies.append(pltpu.make_async_copy(gives[i].at[seat], takes[i].at[seat], own_sem.at[i]))
        copies[-1].start()
    for copy in copies:
        copy.wait()


def reshard(arrays, g, collective_id):
    count = len(arrays)
    return pl.pallas_call(
        functools.partial(reshard_kernel, g),
        in_specs=[pl.BlockSpec(memory_space=pltpu.VMEM)] * count,
        out_specs=[pl.BlockSpec(memory_space=pltpu.VMEM)] * count,
        out_shape=[jax.ShapeDtypeStruct(a.shape, a.dtype) for a in arrays],
        scratch_shapes=[
            pltpu.SemaphoreType.DMA((count, g)),
            pltpu.SemaphoreType.DMA((count, g)),
            pltpu.SemaphoreType.DMA((count,)),
        ],
        compiler_params=pltpu.CompilerParams(
            collective_id=collective_id, has_side_effects=True
        ),
        cost_estimate=pl.CostEstimate(flops=10**8, bytes_accessed=10**8, transcendentals=0),
        name="reshard",
    )(*arrays)


def project_kernel(local_ref, reach_ref, enter_ref, gain_ref, gate_ref, weight_ref, out_ref, total):
    head = pl.program_id(0)
    mix = (
        local_ref[...]
        + dot_nt(reach_ref[0], enter_ref[0, 0])
        + dot_nt(reach_ref[1], enter_ref[1, 0])
    )
    scale = lax.rsqrt(jnp.mean(mix * mix, axis=-1, keepdims=True) + NORM_EPS)
    gate = silu(gate_ref[...].astype(jnp.float32))
    mixed = (mix * scale * gain_ref[...].astype(jnp.float32) * gate).astype(jnp.bfloat16)
    term = dot_nn(mixed, weight_ref[...])

    @pl.when(head == 0)
    def _():
        total[...] = term

    @pl.when(head > 0)
    def _():
        total[...] += term

    @pl.when(head == pl.num_programs(0) - 1)
    def _():
        out_ref[...] = total[...].astype(jnp.bfloat16)


def project(local, reach, entered, gain, gate_logits, weight):
    rows, columns = local.shape
    heads, width = entered.shape[1], entered.shape[3]
    model = weight.shape[1]
    by_head = pl.BlockSpec((rows, width), lambda h: (0, h))
    return pl.pallas_call(
        project_kernel,
        grid=(heads,),
        in_specs=[
            by_head,
            pl.BlockSpec((2, rows, width), lambda h: (0, 0, h)),
            pl.BlockSpec((2, 1, width, width), lambda h: (0, h, 0, 0)),
            pl.BlockSpec((1, width), lambda h: (0, 0)),
            by_head,
            pl.BlockSpec((width, model), lambda h: (h, 0)),
        ],
        out_specs=pl.BlockSpec((rows, model), lambda h: (0, 0)),
        out_shape=jax.ShapeDtypeStruct((rows, model), jnp.bfloat16),
        scratch_shapes=[pltpu.VMEM((rows, model), jnp.float32)],
        cost_estimate=pl.CostEstimate(
            flops=2 * rows * columns * model, bytes_accessed=2 * columns * model, transcendentals=rows * columns
        ),
        name="project",
    )(local, reach, entered, gain.reshape(1, width), gate_logits, weight)


def local(
    queries,
    forget_logits,
    value_matrix,
    output_gate_logits,
    forget_slack,
    spike_log_forget,
    head_norm_gain,
    output_weight,
    residual,
    mixer_norm_gain,
    mixer_gate_weight,
    mixer_up_weight,
    mixer_down_weight,
):
    n, tp = lax.axis_size("sp"), lax.axis_size("tp")
    g = GROUP
    row_count = queries.shape[0]
    depth, units = mixer_gate_weight.shape
    near = [[b * g + j for j in range(g)] for b in range(n // g)]
    far = [[b * g + j for b in range(n // g)] for j in range(g)]

    def cut(weight):
        return weight.reshape(depth, g, units // g).transpose(1, 0, 2)

    pieces = reshard([cut(mixer_gate_weight), cut(mixer_up_weight), cut(mixer_down_weight.T)], g, 2)
    gate_weight, up_weight, down_weight = (
        lax.all_gather(
            p.reshape(g * depth, units // g), "sp", axis=0, tiled=True, axis_index_groups=far
        )
        for p in pieces
    )

    local_out, reach, states = sweep(
        queries, forget_logits, value_matrix, forget_slack, spike_log_forget
    )
    entered = exchange(states)
    part = project(local_out, reach, entered, head_norm_gain, output_gate_logits, output_weight)
    part_rows = row_count // tp
    if tp > 1:
        part = lax.psum_scatter(part, "tp", scatter_dimension=0, tiled=True)
        residual = lax.dynamic_slice_in_dim(
            residual, lax.axis_index("tp") * part_rows, part_rows, 0
        )
    hidden = (residual.astype(jnp.float32) + part.astype(jnp.float32)).astype(jnp.bfloat16)
    hidden_f = hidden.astype(jnp.float32)
    normed = (
        hidden_f
        * lax.rsqrt(jnp.mean(hidden_f * hidden_f, axis=-1, keepdims=True) + NORM_EPS)
        * mixer_norm_gain.astype(jnp.float32)
    ).astype(jnp.bfloat16)
    normed = lax.all_gather(normed, "sp", axis=0, tiled=True, axis_index_groups=near)
    if tp > 1:
        normed = lax.all_gather(normed, "tp", axis=0, tiled=True)
    gate_act = dot_nn(normed, gate_weight)
    up_act = dot_nn(normed, up_weight)
    inner = (silu(gate_act) * up_act).astype(jnp.bfloat16)
    lowered = dot_nt(inner, down_weight).astype(jnp.bfloat16)
    if tp > 1:
        lowered = lax.psum_scatter(lowered, "tp", scatter_dimension=0, tiled=True)
    (terms,) = reshard([lowered.reshape(g, part_rows, lowered.shape[1])], g, 3)
    added = jnp.sum(terms.astype(jnp.float32), axis=0)
    return (hidden_f + added).astype(jnp.bfloat16)


def solution(mesh):
    placed = (
        P("sp", "tp"),
        P(None, "sp", "tp"),
        P("sp", "tp"),
        P("sp", "tp"),
        P("tp"),
        P("sp", "tp"),
        P(),
        P("tp", None),
        P("sp", None),
        P(),
        P("sp", "tp"),
        P("sp", "tp"),
        P("tp", "sp"),
    )
    return jax.shard_map(
        local, mesh=mesh, in_specs=placed, out_specs=P(("sp", "tp"), None), check_vma=False
    )
```

time: 732 us -> 421 us (0.58)
  waiting for transfers between devices: 473 us -> 173 us
  Pallas kernels: 0 us -> 201 us
  blocking collectives: 83.5 us -> 0 us
  other arithmetic: 67.5 us -> 7.38 us
  matrix products: 67.4 us -> 17.8 us
  local copies, waits for them, and re-layouts: 21.9 us -> 6.56 us
    all_gather x5 -> x4, waiting for transfers between devices: 471 us -> 172 us  [the longest x3 122 us: local(): lax.all_gather(p.reshape(g * depth, units // g), 'sp', axis=0, tiled=True...]
    pallas_call x0 -> x5, Pallas kernels: none -> 201 us  [the longest x2 86.9 us: reshard(): pl.pallas_call(functools.partial(reshard_kernel, g), in_specs=[pl.BlockSp...]
    all_gather x2 -> x0, blocking collectives: 83.5 us -> none  [entering(): lax.all_gather(a.astype(kind), axis)]
    add x32 -> x0, other arithmetic: 51.4 us -> none  [the longest x31 48.2 us: chain(): latter[0][..., None] * earlier[1] + latter[1]]
    dot_general x13 -> x2, matrix products: 67.4 us -> 17.8 us  [the longest x1 11.9 us: dot_nt(): lax.dot_general(a, b, (((1,), (1,)), ((), ())), preferred_element_type=jn...]
    rev x3 -> x0, local copies, waits for them, and re-layouts: 11.9 us -> none  [reverse_rows(): return jnp.flip(tensor, 0)]
    mul x6 -> x0, other arithmetic: 9.79 us -> none  [the longest x2 6.45 us: advance(): key_seg * jnp.exp(final_log[None] - running)]
  transfers between devices with their start and end apart: 5 -> 4, of which waited for: 5 -> 3; matrix products, arithmetic and copies ran while one was open for 15% -> 2% of each run, Pallas kernels for 0% -> 27%
where the time goes in v1:
time: 421 us; the launch traced here: 420 us
  Pallas kernels  201 us (48%)
  waiting for transfers between devices  173 us (41%)
  matrix products  17.8 us (4%)
  between operations  13.3 us (3%)
  other arithmetic  7.38 us (2%)
  local copies, waits for them, and re-layouts  6.56 us (2%)
    all_gather x3, waiting for transfers between devices, local(): lax.all_gather(p.reshape(g * depth, units // g), 'sp', axis=0, tiled=True...  122 us
    pallas_call x2, Pallas kernels, reshard(): pl.pallas_call(functools.partial(reshard_kernel, g), in_specs=[pl.BlockSp...  86.9 us
    pallas_call x1, Pallas kernels, exchange(): pl.pallas_call(functools.partial(exchange_kernel, n), in_specs=[pl.BlockS...  83.1 us
    all_gather x1, waiting for transfers between devices, local(): lax.all_gather(normed, 'sp', axis=0, tiled=True, axis_index_groups=near)  49.7 us
    pallas_call x1, Pallas kernels, project(): pl.pallas_call(project_kernel, grid=(heads,), in_specs=[by_head, pl.Block...  16.6 us
    pallas_call x1, Pallas kernels, sweep(): pl.pallas_call(sweep_kernel, grid=(heads,), in_specs=[by_head, pl.BlockSp...  14.8 us
    dot_general x1, matrix products, dot_nt(): lax.dot_general(a, b, (((1,), (1,)), ((), ())), preferred_element_type=jn...  11.9 us
  transfers between devices with their start and end apart: 4, of which 3 were waited for; matrix products, arithmetic and copies ran while one was open for 2% of the time, Pallas kernels for 27%

profile of v1, /device:TPU:1, one launch (start us, length us, event | category | flops | bytes accessed | tf_op | source)
XLA Modules:
  0.0 419.6 jit_solution(11957039191342917007)
XLA Ops:
  6.5 0.0 copy-start.2
  6.5 0.0 copy-start.3
  6.5 0.0 all-gather.7.cloned.1.call-start
  6.5 2.0 reshape.46
  8.5 1.0 copy.22
  9.5 0.0 copy-done.2
  9.5 0.7 reshape.47
  10.2 0.0 copy-done.3
  10.2 0.7 reshape.48
  10.9 0.0 copy-start.5
  10.9 0.0 copy-start.4
  10.9 1.5 copy_bitcast_fusion
  12.4 33.6 %reshard.2 = (bf16[8,64,704]{2,1,0:T(8,128)(2,1)}, bf16[8,64,704]{2,1,0:T(8,128)(2,1)}, bf16[8,64,704]{2,1,0:T(8,128)(2,1)}) custom-call(bf16[8,64,704]{2,1,0:T(8,128)(2,1)} %bitcast.23, bf16[8,64,704]{2,1,0:T(8,128)(2,1)} %get-tuple-element.18.refs_1_, bf16[8,64,704]{2,1,0:T(8,128)(2,1)} %get-tuple-element.17.refs_2_), custom_call_target="tpu_custom_call" | custom-call | flops 100000000 | bytes 100000000 | tf_op jit(solution)/shard_map/reshard/pallas_call | solution.py:248
  46.0 0.0 all-gather.7.cloned.1.call-update
  46.0 0.0 all-gather.5.cloned.1.call-start
  46.1 0.0 copy-done.5
  46.1 0.0 copy-done.4
  46.1 0.7 copy.15.spike_ref
  46.8 14.8 %sweep.1 = (f32[128,2048]{1,0:T(8,128)}, bf16[2,128,2048]{2,1,0:T(8,128)(2,1)}, bf16[2,16,144,128]{3,2,1,0:T(8,128)(2,1)}) custom-call(bf16[128,2048]{1,0:T(8,128)(2,1)} %q_ref.1, bf16[2,128,2048]{2,1,0:T(8,128)(2,1)} %f_ref.1, bf16[128,2048]{1,0:T(8,128)(2,1)} %v_ref.1, f32[1,2048]{1,0:T(1,128)} %bitcast.30, f32[128,16]{1,0:T(8,128)} %copy.15.spike_ref), custom_call_target="tpu_custom_call" | custom-call | flops 671088640 | bytes 2097152 | tf_op jit(solution)/shard_map/sweep/pallas_call | solution.py:79
  61.6 83.1 %exchange.1 = bf16[32,128,128]{2,1,0:T(8,128)(2,1)} custom-call(bf16[32,144,128]{2,1,0:T(8,128)(2,1)} %bitcast.24), custom_call_target="tpu_custom_call" | custom-call | flops 100000000 | bytes 100000000 | tf_op jit(solution)/shard_map/exchange/pallas_call | solution.py:192
  144.8 0.0 copy-start.1
  144.8 16.6 %project.1 = bf16[128,2048]{1,0:T(8,128)(2,1)} custom-call(f32[128,2048]{1,0:T(8,128)} %get-tuple-element.11.local_ref, bf16[2,128,2048]{2,1,0:T(8,128)(2,1)} %get-tuple-element.12.reach_ref, bf16[2,16,128,128]{3,2,1,0:T(8,128)(2,1)} %bitcast.21, bf16[1,128]{1,0:T(2,128)(2,1)} %bitcast.29, bf16[128,2048]{1,0:T(8,128)(2,1)} %gate_ref.1, ...), custom_call_target="tpu_custom_call" | custom-call | flops 1073741824 | bytes 8388608 | tf_op jit(solution)/shard_map/project/pallas_call | solution.py:296
  161.3 0.0 copy-done.1
  161.3 1.3 fusion
  162.6 2.0 fusion.2
  164.7 0.0 all-gather.5.cloned.1.call-update
  164.7 0.0 all-gather.9.cloned.1.call-start
  164.7 0.7 all-gather.9.cloned.1.call-update
  165.4 0.0 all-gather.11.cloned.1.call-start
  165.5 0.5 all-gather.11.cloned.1.call-update
  166.0 0.0 all-gather.7.cloned.1.call-done
  166.0 49.7 %all-gather.5.cloned.1.call-done = bf16[1024,2048]{1,0:T(8,128)(2,1)} async-done(((bf16[128,2048]{1,0:T(8,128)(2,1)}), bf16[1024,2048]{1,0:T(8,128)(2,1)}) %all-gather.5.cloned.1.call-update) | async-done | bytes 4194320 | tf_op jit(solution)/shard_map/all_gather | solution.py:368
  215.8 5.9 %fusion.5 = f32[1024,704]{0,1:T(8,128)S(1)} fusion(bf16[1024,2048]{1,0:T(8,128)(2,1)} %all-gather.5.cloned.1.call-done, bf16[2048,704]{1,0:T(8,128)(2,1)} %all-gather.7.cloned.1.call-done), kind=kOutput, calls=%fused_computation.16 | convolution fusion | flops 2952790016 | bytes 9961472 | tf_op jit(solution)/shard_map/dot_general | solution.py:25
  221.7 58.5 %all-gather.9.cloned.1.call-done = bf16[2048,704]{1,0:T(8,128)(2,1)} async-done(((bf16[512,704]{1,0:T(8,128)(2,1)}), bf16[2048,704]{1,0:T(8,128)(2,1)}) %all-gather.9.cloned.1.call-update) | async-done | bytes 2883600 | tf_op jit(solution)/shard_map/all_gather | solution.py:344
  280.2 63.5 %all-gather.11.cloned.1.call-done = bf16[2048,704]{1,0:T(8,128)(2,1)} async-done(((bf16[512,704]{1,0:T(8,128)(2,1)}), bf16[2048,704]{1,0:T(8,128)(2,1)}) %all-gather.11.cloned.1.call-update) | async-done | bytes 2883600 | tf_op jit(solution)/shard_map/all_gather | solution.py:344
  343.8 11.9 %convolution_convert_fusion = bf16[1024,2048]{1,0:T(8,128)(2,1)} fusion(bf16[2048,704]{1,0:T(8,128)(2,1)} %all-gather.11.cloned.1.call-done, f32[1024,704]{0,1:T(8,128)S(1)} %fusion.5, bf16[1024,2048]{1,0:T(8,128)(2,1)} %all-gather.5.cloned.1.call-done, bf16[2048,704]{1,0:T(8,128)(2,1)} %all-gather.9.cloned.1.call-done), kind=kOutput, calls=%fused_computation.1 | convolution fusion | flops 5912002560 | bytes 17039360 | tf_op jit(solution)/shard_map/dot_general | solution.py:17
  355.7 53.3 %reshard.3 = bf16[8,128,2048]{2,1,0:T(8,128)(2,1)} custom-call(bf16[8,128,2048]{2,1,0:T(8,128)(2,1)} %bitcast.22), custom_call_target="tpu_custom_call" | custom-call | flops 100000000 | bytes 100000000 | tf_op jit(solution)/shard_map/reshard/pallas_call | solution.py:248
  409.0 0.0 copy-start
  409.0 3.0 convert_reduce_fusion
  412.1 0.0 copy-done
  412.1 1.0 fusion.3
  (2 shorter events, 0.0 us)
Async XLA Ops:
  6.5 3.0 copy-start.2
  6.5 3.7 copy-start.3
  6.5 159.5 %all-gather.7.cloned.1.call-start = ((), (), s32[]{:S(2)}) async-start(), calls=%async_computation.1 | async-start | bytes 3932160 | tf_op jit(solution)/shard_map/all_gather | solution.py:344
  10.9 35.2 %copy-start.5 = (bf16[2048]{0:T(1024)(128)(2,1)S(1)}, bf16[2048]{0:T(1024)(128)(2,1)}, u32[]{:S(2)}) copy-start(bf16[2048]{0:T(1024)(128)(2,1)} %param.22) | copy-start | bytes 12292
  10.9 35.2 %copy-start.4 = (f32[128,16]{0,1:T(8,128)S(1)}, f32[128,16]{0,1:T(8,128)}, u32[]{:S(2)}) copy-start(f32[128,16]{0,1:T(8,128)} %param.18) | copy-start | bytes 24580
  46.0 169.7 %all-gather.5.cloned.1.call-start = ((), (), s32[]{:S(2)}) async-start(), calls=%async_computation | async-start | bytes 4718592 | tf_op jit(solution)/shard_map/all_gather | solution.py:368
  144.8 16.6 %copy-start.1 = (bf16[128,2048]{1,0:T(8,128)(2,1)S(1)}, bf16[128,2048]{1,0:T(8,128)(2,1)}, u32[]{:S(2)}) copy-start(bf16[128,2048]{1,0:T(8,128)(2,1)} %param.21) | copy-start | bytes 1572868
  164.7 115.5 %all-gather.9.cloned.1.call-start = ((), (), s32[]{:S(2)}) async-start(), calls=%async_computation.2 | async-start | bytes 3932160 | tf_op jit(solution)/shard_map/all_gather | solution.py:344
  165.4 178.3 %all-gather.11.cloned.1.call-start = ((), (), s32[]{:S(2)}) async-start(), calls=%async_computation.3 | async-start | bytes 3932160 | tf_op jit(solution)/shard_map/all_gather | solution.py:344
  409.0 3.1 copy-start
Sparse Core Ops, SparseCore 0:
  46.1 106.3 all-gather.6
  164.8 50.8 all-gather.4
  217.3 62.8 all-gather.8
  281.7 62.0 all-gather.10

commit v2 on v1

--- a/solution.py
+++ b/solution.py
@@ -203,7 +203,6 @@
             pltpu.SemaphoreType.DMA((n,)),
         ],
         compiler_params=pltpu.CompilerParams(collective_id=1, has_side_effects=True),
-        cost_estimate=pl.CostEstimate(flops=10**8, bytes_accessed=10**8, transcendentals=0),
         name="exchange",
     )(states.reshape(n, rows + PAD_ROWS, width))
     return entered.reshape(ways, heads, depth, width)
@@ -258,9 +257,49 @@
         compiler_params=pltpu.CompilerParams(
             collective_id=collective_id, has_side_effects=True
         ),
-        cost_estimate=pl.CostEstimate(flops=10**8, bytes_accessed=10**8, transcendentals=0),
         name="reshard",
     )(*arrays)
+
+
+def gather_kernel(g, give, take, out_sem, in_sem):
+    me = lax.axis_index("sp")
+    base = me // g * g
+    seat = me - base
+
+    def other(k):
+        return lax.rem(seat + k, g)
+
+    greet("sp", lambda k: base + other(k), g)
+    copies = []
+    for k in range(1, g):
+        copies.append(
+            pltpu.make_async_remote_copy(
+                src_ref=give,
+                dst_ref=take.at[seat],
+                send_sem=out_sem.at[k],
+                recv_sem=in_sem.at[k],
+                device_id={"sp": base + other(k)},
+                device_id_type=MESH,
+            )
+        )
+        copies[-1].start()
+    take[seat] = give[...]
+    for copy in copies:
+        copy.wait()
+
+
+def gather(array, g, collective_id):
+    return pl.pallas_call(
+        functools.partial(gather_kernel, g),
+        in_specs=[pl.BlockSpec(memory_space=pltpu.VMEM)],
+        out_specs=pl.BlockSpec(memory_space=pltpu.VMEM),
+        out_shape=jax.ShapeDtypeStruct((g,) + array.shape, array.dtype),
+        scratch_shapes=[pltpu.SemaphoreType.DMA((g,)), pltpu.SemaphoreType.DMA((g,))],
+        compiler_params=pltpu.CompilerParams(
+            collective_id=collective_id, has_side_effects=True
+        ),
+        name="gather",
+    )(array).reshape((g * array.shape[0],) + array.shape[1:])
 
 
 def project_kernel(local_ref, reach_ref, enter_ref, gain_ref, gate_ref, weight_ref, out_ref, total):
@@ -333,7 +372,6 @@
     g = GROUP
     row_count = queries.shape[0]
     depth, units = mixer_gate_weight.shape
-    near = [[b * g + j for j in range(g)] for b in range(n // g)]
     far = [[b * g + j for b in range(n // g)] for j in range(g)]
 
     def cut(weight):
@@ -365,7 +403,7 @@
         * lax.rsqrt(jnp.mean(hidden_f * hidden_f, axis=-1, keepdims=True) + NORM_EPS)
         * mixer_norm_gain.astype(jnp.float32)
     ).astype(jnp.bfloat16)
-    normed = lax.all_gather(normed, "sp", axis=0, tiled=True, axis_index_groups=near)
+    normed = gather(normed, g, 4)
     if tp > 1:
         normed = lax.all_gather(normed, "tp", axis=0, tiled=True)
     gate_act = dot_nn(normed, gate_weight)

time: 421 us -> 359 us (0.85)
  waiting for transfers between devices: 173 us -> 47.6 us
  Pallas kernels: 201 us -> 264 us
    all_gather x3, waiting for transfers between devices: 122 us -> 46.2 us  [local(): lax.all_gather(p.reshape(g * depth, units // g), 'sp', axis=0, tiled=True...]
    pallas_call x0 -> x1, Pallas kernels: none -> 54.7 us  [gather(): pl.pallas_call(functools.partial(gather_kernel, g), in_specs=[pl.BlockSpe...]
    all_gather x1 -> x0, waiting for transfers between devices: 49.7 us -> none  [local(): lax.all_gather(normed, 'sp', axis=0, tiled=True, axis_index_groups=near)]
    pallas_call x1, Pallas kernels: 83.1 us -> 91.2 us  [exchange(): pl.pallas_call(functools.partial(exchange_kernel, n), in_specs=[pl.BlockS...]
  transfers between devices with their start and end apart: 4 -> 3, of which waited for: 3 -> 1; matrix products, arithmetic and copies ran while one was open for 2% -> 3% of each run, Pallas kernels for 27% -> 50%
where the time goes in v2:
time: 359 us; the launch traced here: 357 us
  Pallas kernels  264 us (74%)
  waiting for transfers between devices  47.6 us (13%)
  matrix products  17.9 us (5%)
  between operations  13.3 us (4%)
  other arithmetic  7.38 us (2%)
  local copies, waits for them, and re-layouts  6.58 us (2%)
    pallas_call x1, Pallas kernels, exchange(): pl.pallas_call(functools.partial(exchange_kernel, n), in_specs=[pl.BlockS...  91.2 us
    pallas_call x2, Pallas kernels, reshard(): pl.pallas_call(functools.partial(reshard_kernel, g), in_specs=[pl.BlockSp...  86.9 us
    pallas_call x1, Pallas kernels, gather(): pl.pallas_call(functools.partial(gather_kernel, g), in_specs=[pl.BlockSpe...  54.7 us
    all_gather x3, waiting for transfers between devices, local(): lax.all_gather(p.reshape(g * depth, units // g), 'sp', axis=0, tiled=True...  46.2 us
    pallas_call x1, Pallas kernels, project(): pl.pallas_call(project_kernel, grid=(heads,), in_specs=[by_head, pl.Block...  16.6 us
    pallas_call x1, Pallas kernels, sweep(): pl.pallas_call(sweep_kernel, grid=(heads,), in_specs=[by_head, pl.BlockSp...  14.8 us
    dot_general x1, matrix products, dot_nt(): lax.dot_general(a, b, (((1,), (1,)), ((), ())), preferred_element_type=jn...  11.9 us
  transfers between devices with their start and end apart: 3, of which 1 were waited for; matrix products, arithmetic and copies ran while one was open for 3% of the time, Pallas kernels for 50%

profile of v2, /device:TPU:1, one launch (start us, length us, event | category | flops | bytes accessed | tf_op | source)
XLA Modules:
  0.0 357.1 jit_solution(7320738690922416834)
XLA Ops:
  6.5 0.0 copy-start.2
  6.5 0.0 copy-start.3
  6.5 0.0 all-gather.4.cloned.1.call-start
  6.5 2.0 reshape.50
  8.5 1.0 copy.22
  9.5 0.0 copy-done.2
  9.5 0.7 reshape.51
  10.2 0.0 copy-done.3
  10.2 0.7 reshape.52
  10.9 1.5 copy_bitcast_fusion
  12.4 0.0 copy-start.5
  12.4 0.0 copy-start.4
  12.4 33.6 %reshard.2 = (bf16[8,64,704]{2,1,0:T(8,128)(2,1)}, bf16[8,64,704]{2,1,0:T(8,128)(2,1)}, bf16[8,64,704]{2,1,0:T(8,128)(2,1)}) custom-call(bf16[8,64,704]{2,1,0:T(8,128)(2,1)} %bitcast.26, bf16[8,64,704]{2,1,0:T(8,128)(2,1)} %get-tuple-element.18.refs_1_, bf16[8,64,704]{2,1,0:T(8,128)(2,1)} %get-tuple-element.17.refs_2_), custom_call_target="tpu_custom_call" | custom-call | tf_op jit(solution)/shard_map/reshard/pallas_call | solution.py:247
  46.0 0.0 all-gather.4.cloned.1.call-update
  46.1 0.0 all-gather.6.cloned.1.call-start
  46.1 0.7 all-gather.6.cloned.1.call-update
  46.8 0.0 all-gather.8.cloned.1.call-start
  46.9 0.7 all-gather.8.cloned.1.call-update
  47.5 0.0 copy-done.5
  47.6 0.0 copy-done.4
  47.6 0.7 copy.15.spike_ref
  48.3 14.8 %sweep.1 = (f32[128,2048]{1,0:T(8,128)}, bf16[2,128,2048]{2,1,0:T(8,128)(2,1)}, bf16[2,16,144,128]{3,2,1,0:T(8,128)(2,1)}) custom-call(bf16[128,2048]{1,0:T(8,128)(2,1)} %q_ref.1, bf16[2,128,2048]{2,1,0:T(8,128)(2,1)} %f_ref.1, bf16[128,2048]{1,0:T(8,128)(2,1)} %v_ref.1, f32[1,2048]{1,0:T(1,128)} %bitcast.33, f32[128,16]{1,0:T(8,128)} %copy.15.spike_ref), custom_call_target="tpu_custom_call" | custom-call | flops 671088640 | bytes 2097152 | tf_op jit(solution)/shard_map/sweep/pallas_call | solution.py:79
  63.1 91.2 %exchange.1 = bf16[32,128,128]{2,1,0:T(8,128)(2,1)} custom-call(bf16[32,144,128]{2,1,0:T(8,128)(2,1)} %bitcast.27), custom_call_target="tpu_custom_call" | custom-call | tf_op jit(solution)/shard_map/exchange/pallas_call | solution.py:192
  154.3 0.0 copy-start.1
  154.3 16.6 %project.1 = bf16[128,2048]{1,0:T(8,128)(2,1)} custom-call(f32[128,2048]{1,0:T(8,128)} %get-tuple-element.11.local_ref, bf16[2,128,2048]{2,1,0:T(8,128)(2,1)} %get-tuple-element.12.reach_ref, bf16[2,16,128,128]{3,2,1,0:T(8,128)(2,1)} %bitcast.22, bf16[1,128]{1,0:T(2,128)(2,1)} %bitcast.32, bf16[128,2048]{1,0:T(8,128)(2,1)} %gate_ref.1, ...), custom_call_target="tpu_custom_call" | custom-call | flops 1073741824 | bytes 8388608 | tf_op jit(solution)/shard_map/project/pallas_call | solution.py:335
  170.9 0.0 copy-done.1
  170.9 1.3 fusion
  172.2 2.0 fusion.2.give
  174.3 54.7 %gather.1 = bf16[8,128,2048]{2,1,0:T(8,128)(2,1)} custom-call(bf16[128,2048]{1,0:T(8,128)(2,1)} %fusion.2.give), custom_call_target="tpu_custom_call" | custom-call | tf_op jit(solution)/shard_map/gather/pallas_call | solution.py:292
  229.0 0.0 all-gather.4.cloned.1.call-done
  229.0 6.0 %fusion.5 = f32[1024,704]{0,1:T(8,128)S(1)} fusion(bf16[1024,2048]{1,0:T(8,128)(2,1)} %bitcast.23, bf16[2048,704]{1,0:T(8,128)(2,1)} %all-gather.4.cloned.1.call-done), kind=kOutput, calls=%fused_computation.16 | convolution fusion | flops 2952790016 | bytes 9961472 | tf_op jit(solution)/shard_map/dot_general | solution.py:25
  235.0 0.0 all-gather.6.cloned.1.call-done
  235.0 46.2 %all-gather.8.cloned.1.call-done = bf16[2048,704]{1,0:T(8,128)(2,1)} async-done(((bf16[512,704]{1,0:T(8,128)(2,1)}), bf16[2048,704]{1,0:T(8,128)(2,1)}) %all-gather.8.cloned.1.call-update) | async-done | bytes 2883600 | tf_op jit(solution)/shard_map/all_gather | solution.py:382
  281.2 11.9 %convolution_convert_fusion = bf16[1024,2048]{1,0:T(8,128)(2,1)} fusion(bf16[2048,704]{1,0:T(8,128)(2,1)} %all-gather.8.cloned.1.call-done, f32[1024,704]{0,1:T(8,128)S(1)} %fusion.5, bf16[1024,2048]{1,0:T(8,128)(2,1)} %bitcast.24, bf16[2048,704]{1,0:T(8,128)(2,1)} %all-gather.6.cloned.1.call-done), kind=kOutput, calls=%fused_computation.1 | convolution fusion | flops 5912002560 | bytes 17039360 | tf_op jit(solution)/shard_map/dot_general | solution.py:17
  293.1 53.3 %reshard.3 = bf16[8,128,2048]{2,1,0:T(8,128)(2,1)} custom-call(bf16[8,128,2048]{2,1,0:T(8,128)(2,1)} %bitcast.25), custom_call_target="tpu_custom_call" | custom-call | tf_op jit(solution)/shard_map/reshard/pallas_call | solution.py:247
  346.5 0.0 copy-start
  346.5 3.0 convert_reduce_fusion
  349.5 0.0 copy-done
  349.5 1.0 fusion.3
  (2 shorter events, 0.0 us)
Async XLA Ops:
  6.5 3.0 copy-start.2
  6.5 3.7 %copy-start.3 = (bf16[5632,64]{0,1:T(8,128)(2,1)S(1)}, bf16[5632,64]{0,1:T(8,128)(2,1)}, u32[]{:S(2)}) copy-start(bf16[5632,64]{0,1:T(8,128)(2,1)} %param.25) | copy-start | bytes 2162692
  6.5 222.5 %all-gather.4.cloned.1.call-start = ((), (), s32[]{:S(2)}) async-start(), calls=%async_computation | async-start | bytes 3932160 | tf_op jit(solution)/shard_map/all_gather | solution.py:382
  12.4 35.1 %copy-start.5 = (bf16[2048]{0:T(1024)(128)(2,1)S(1)}, bf16[2048]{0:T(1024)(128)(2,1)}, u32[]{:S(2)}) copy-start(bf16[2048]{0:T(1024)(128)(2,1)} %param.22) | copy-start | bytes 12292
  12.4 35.2 %copy-start.4 = (f32[128,16]{0,1:T(8,128)S(1)}, f32[128,16]{0,1:T(8,128)}, u32[]{:S(2)}) copy-start(f32[128,16]{0,1:T(8,128)} %param.18) | copy-start | bytes 24580
  46.1 189.0 %all-gather.6.cloned.1.call-start = ((), (), s32[]{:S(2)}) async-start(), calls=%async_computation.1 | async-start | bytes 3932160 | tf_op jit(solution)/shard_map/all_gather | solution.py:382
  46.8 234.4 %all-gather.8.cloned.1.call-start = ((), (), s32[]{:S(2)}) async-start(), calls=%async_computation.2 | async-start | bytes 3932160 | tf_op jit(solution)/shard_map/all_gather | solution.py:382
  154.3 16.7 %copy-start.1 = (bf16[128,2048]{1,0:T(8,128)(2,1)S(1)}, bf16[128,2048]{1,0:T(8,128)(2,1)}, u32[]{:S(2)}) copy-start(bf16[128,2048]{1,0:T(8,128)(2,1)} %param.21) | copy-start | bytes 1572868
  346.5 3.1 copy-start
Sparse Core Ops, SparseCore 0:
  46.2 106.6 all-gather.3
  154.4 63.0 all-gather.5
  219.1 62.0 all-gather.7
